TPU v7x, 32 devices: a whole 2x2x4 slice. The times are simulated.
32 devices in a mesh: grp: 2 (over y), fs: 4 (over z), tp: 4 (over x, core).
Axes of the slice: x: 2, y: 2, z: 4, core: 2. Of those that a mesh axis runs over, the one named last changes fastest.
Arguments:
- tokens: bfloat16 [2048, 2048], P(('grp', 'fs')), parts along dimension 0, may hold values from -6 to 6
- norm_gain: float32 [2048], P('fs'), may hold values from 0.1 to 1.9
- gate_master: float32 [4, 2048, 1024], P(None, 'fs', 'tp'), may hold values from -0.125 to 0.125
- up_master: float32 [4, 2048, 1024], P(None, 'fs', 'tp'), may hold values from -0.125 to 0.125
- chosen: int32 [2048, 2], P(('grp', 'fs')), parts along dimension 0, may hold values from 0 to 3, all different within a row; in each aligned block of 256 rows (0 to 255, 256 to 511, ...) at most 256 rows name the same one
- affinity: float32 [2048, 2], P(('grp', 'fs')), parts along dimension 0, may hold values from 0.05 to 1
Outputs:
- gate_served: bfloat16 [8, 2048, 1024], P(('grp', 'fs'), None, 'tp'), parts along dimension 0
- up_served: bfloat16 [8, 2048, 1024], P(('grp', 'fs'), None, 'tp'), parts along dimension 0
- hidden: bfloat16 [2048, 2, 1024], P(('grp', 'fs'), None, 'tp'), parts along dimension 0
There are 2 independent parts, one for each index of `grp`. A program takes and returns all parts, laid end to end along the dimension named above; an argument that names none is the same for every part. Nothing has to cross between parts.
Inputs may be any that keep to these rules, and one draw needn't show every extreme that they name: Among the rows of one index of fs (256 tokens, all their choices) no expert is chosen more than 256 times, a bound that some block reaches; the choices of one token differ.
All inputs are finite; a program needn't handle non-finite values.
Results may differ from a plain program's by a relative error of at most 0.023.
Values may be sent and summed in bfloat16 or wider, within the bound.
A program may use at most 64 MiB of HBM per device.

v0:
```python
import jax
import jax.numpy as jnp
from jax import lax
from jax.sharding import PartitionSpec as P


def on_device(tokens, norm_gain, gate_master, up_master, chosen, affinity):
    folded_gate = (gate_master * norm_gain[None, :, None]).astype(jnp.bfloat16)
    folded_up = (up_master * norm_gain[None, :, None]).astype(jnp.bfloat16)
    new_gate, new_up = (
        lax.all_to_all(folded_gate, "fs", split_axis=0, concat_axis=1, tiled=True),
        lax.all_to_all(folded_up, "fs", split_axis=0, concat_axis=1, tiled=True),
    )
    experts_all = gate_master.shape[0]
    tok_rows, width = tokens.shape
    top = chosen.shape[1]
    capacity = tok_rows * top * 2 // experts_all
    local = new_gate.shape[0]
    xfloat = tokens.astype(jnp.float32)
    scale = lax.rsqrt(jnp.mean(xfloat * xfloat, axis=-1) + 1e-06)
    share = affinity / jnp.sum(affinity, axis=-1, keepdims=True)
    flat_e = chosen.reshape(-1)
    onehot = (flat_e[:, None] == jnp.arange(experts_all, dtype=jnp.int32)[None, :]).astype(
        jnp.int32
    )
    slot = jnp.sum((jnp.cumsum(onehot, axis=0) - onehot) * onehot, axis=1)
    target = flat_e * capacity + slot
    owner = jnp.repeat(jnp.arange(tok_rows, dtype=jnp.int32), top)
    total = experts_all * capacity
    scale_buf = (
        jnp.zeros((total,), jnp.float32).at[target].set(scale[owner]).reshape(experts_all, capacity)
    )
    share_buf = (
        jnp.zeros((total,), jnp.float32)
        .at[target]
        .set(share.reshape(-1))
        .reshape(experts_all, capacity)
    )
    narrow = width // lax.axis_size("tp")
    own_cols = lax.dynamic_slice_in_dim(tokens, lax.axis_index("tp") * narrow, narrow, 1)
    row_buf = jnp.zeros((total, narrow), jnp.bfloat16).at[target].set(own_cols[owner])
    row_buf = row_buf.reshape(experts_all, capacity, narrow)
    got_rows, got_scale, got_share = (
        lax.all_to_all(row_buf, "fs", split_axis=0, concat_axis=0, tiled=True),
        lax.all_to_all(
            scale_buf.astype(jnp.bfloat16), "fs", split_axis=0, concat_axis=0, tiled=True
        ).astype(scale_buf.dtype),
        lax.all_to_all(
            share_buf.astype(jnp.bfloat16), "fs", split_axis=0, concat_axis=0, tiled=True
        ).astype(share_buf.dtype),
    )
    sources = got_rows.shape[0] // local
    got_rows = got_rows.reshape(sources, local, capacity, narrow)
    piece = lax.all_gather(got_rows, "tp", axis=3, tiled=True)
    more_gate = jnp.einsum("secd,edf->secf", piece, new_gate, preferred_element_type=jnp.float32)
    more_up = jnp.einsum("secd,edf->secf", piece, new_up, preferred_element_type=jnp.float32)
    gate = more_gate
    up = more_up
    factor = got_scale.reshape(sources, local, capacity)[..., None]
    weight = got_share.reshape(sources, local, capacity)[..., None]
    gate = gate * factor
    up = up * factor
    hidden_rows = (weight * jax.nn.silu(gate) * up).astype(jnp.bfloat16)
    hidden_rows = hidden_rows.reshape(sources * local, capacity, hidden_rows.shape[3])
    back = lax.all_to_all(hidden_rows, "fs", split_axis=0, concat_axis=0, tiled=True)
    picked = back.reshape(total, back.shape[2])[target].reshape(tok_rows, top, back.shape[2])
    return (new_gate, new_up, picked)


def solution(mesh):
    return jax.shard_map(
        on_device,
        mesh=mesh,
        in_specs=(
            P(("grp", "fs"), None),
            P("fs"),
            P(None, "fs", "tp"),
            P(None, "fs", "tp"),
            P(("grp", "fs"), None),
            P(("grp", "fs"), None),
        ),
        out_specs=(
            P(("grp", "fs"), None, "tp"),
            P(("grp", "fs"), None, "tp"),
            P(("grp", "fs"), None, "tp"),
        ),
        check_vma=False,
    )
```

profile of v0, /device:TPU:0, one launch (start us, length us, event | category | flops | bytes accessed | tf_op | source)
XLA Modules:
  0.0 163.8 jit_solution(18356809726918053598)
XLA Ops:
  7.2 0.7 broadcast_multiply_fusion
  7.9 0.8 copy.26
  9.3 1.2 reduce-window.6
  11.2 1.0 constant_dynamic-slice_fusion
  12.2 5.0 %scatter_custom_fusion.1 = bf16[1024,512]{1,0:T(8,128)(2,1)S(1)} fusion(s32[512]{0:T(512)S(1)} %bitcast.83, bf16[256,512]{1,0:T(8,128)(2,1)S(1)} %constant_dynamic-slice_fusion, s32[1024]{0:T(1024)S(1)} %pad_clamp_fusion.1, bf16[]{:T(256)} %constant.15.clone.1), kind=kCustom, calls=%fused_computation.18 | custom fusion | bytes 1048578 | tf_op jit(solution)/shard_map/scatter | solution.py:41
  17.3 32.0 %all_to_all.46 = bf16[4,256,512]{2,1,0:T(8,128)(2,1)} all-to-all(bf16[4,256,512]{2,1,0:T(8,128)(2,1)S(1)} %bitcast.82), channel_id=1, replica_groups=mesh['grp'=2,'fs'=4,'tp'=4] {'fs'}, dimensions={0} | all-to-all | bytes 2097152 | tf_op jit(solution)/shard_map/all_to_all | solution.py:44
  49.6 2.4 %scatter_custom_fusion = f32[1024]{0:T(1024)S(1)} fusion(s32[512]{0:T(512)S(1)} %bitcast.84, f32[512]{0:T(512)S(1)} %reshape.212, f32[]{:T(128)} %constant.11.clone.1), kind=kCustom, calls=%fused_computation.38 | custom fusion | bytes 4100 | tf_op jit(solution)/shard_map/scatter | solution.py:36
  53.9 3.2 %all-to-all-start.2 = ((bf16[4,2,128]{2,1,0:T(2,128)(2,1)}), bf16[4,2,128]{2,1,0:T(2,128)(2,1)S(1)}, u32[]{:S(2)}, u32[]{:S(2)}) async-start(bf16[4,2,128]{2,1,0:T(2,128)(2,1)} %reshape.249), calls=%async_computation.2 | async-start | bytes 4096 | tf_op jit(solution)/shard_map/all_to_all | solution.py:48
  57.4 3.5 %gather_fusion = f32[512]{0:T(512)S(1)} fusion(f32[256]{0:T(256)S(1)} %add_rsqrt_fusion, s32[1024]{0:T(1024)S(1)} %pad_clamp_fusion.1), kind=kCustom, calls=%fused_computation.1 | custom fusion | bytes 6144 | tf_op jit(solution)/shard_map/gather | solution.py:31
  61.0 2.4 %scatter_custom_fusion.2 = f32[1024]{0:T(1024)S(1)} fusion(s32[512]{0:T(512)S(1)} %bitcast.85, f32[512]{0:T(512)S(1)} %gather_fusion, f32[]{:T(128)} %constant.11.clone.1), kind=kCustom, calls=%fused_computation.36 | custom fusion | bytes 4100 | tf_op jit(solution)/shard_map/scatter | solution.py:31
  64.7 5.0 %all-to-all-start.4 = ((bf16[4,2,128]{2,1,0:T(2,128)(2,1)}), bf16[4,2,128]{2,1,0:T(2,128)(2,1)S(1)}, u32[]{:S(2)}, u32[]{:S(2)}) async-start(bf16[4,2,128]{2,1,0:T(2,128)(2,1)} %reshape.247), calls=%async_computation.4 | async-start | bytes 4096 | tf_op jit(solution)/shard_map/all_to_all | solution.py:45
  69.7 3.5 %multiply_convert_fusion = (bf16[4,512,256]{2,1,0:T(8,128)(2,1)}, bf16[4,512,256]{2,1,0:T(8,128)(2,1)S(1)}) fusion(f32[4,512,256]{2,1,0:T(8,128)} %param.9, f32[512]{0:T(512)S(1)} %copy-done.2, f32[4,512,256]{2,1,0:T(8,128)} %param.8), kind=kLoop, calls=%fused_computation.7 | loop fusion | flops 2097152 | bytes 6293504 | tf_op jit(solution)/shard_map/convert_element_type | solution.py:9
  73.3 2.0 %all-to-all-done.4 = bf16[4,2,128]{2,1,0:T(2,128)(2,1)S(1)} async-done(((bf16[4,2,128]{2,1,0:T(2,128)(2,1)}), bf16[4,2,128]{2,1,0:T(2,128)(2,1)S(1)}, u32[]{:S(2)}, u32[]{:S(2)}) %all-to-all-start.4) | async-done | bytes 2080 | tf_op jit(solution)/shard_map/all_to_all | solution.py:45
  75.2 26.7 %all_to_all.47 = bf16[4,512,256]{2,1,0:T(8,128)(2,1)S(1)} all-to-all(bf16[4,512,256]{2,1,0:T(8,128)(2,1)S(1)} %get-tuple-element.4), channel_id=1, replica_groups=mesh['grp'=2,'fs'=4,'tp'=4] {'fs'}, dimensions={0} | all-to-all | bytes 2097152 | tf_op jit(solution)/shard_map/all_to_all | solution.py:11
  101.9 3.7 %all-to-all-start.1 = ((bf16[4,512,256]{2,1,0:T(8,128)(2,1)}), bf16[4,512,256]{2,1,0:T(8,128)(2,1)S(1)}, u32[]{:S(2)}, u32[]{:S(2)}) async-start(bf16[4,512,256]{2,1,0:T(8,128)(2,1)} %get-tuple-element.3), calls=%async_computation.1 | async-start | bytes 2097152 | tf_op jit(solution)/shard_map/all_to_all | solution.py:12
  105.7 3.5 %fusion.3 = f32[4,1,256,256]{2,3,0,1:T(8,128)S(1)} fusion(bf16[2048,256,1]{1,0,2:T(8,128)(2,1)S(1)} %bitcast.78, bf16[4,256,2048]{2,1,0:T(8,128)(2,1)} %all-gather.3.cloned.1.call-done, f32[4,256]{1,0:T(4,128)S(1)} %bitcast.91), kind=kOutput, calls=%fused_computation.14 | convolution fusion | flops 1074003968 | bytes 6295552 | tf_op jit(solution)/shard_map/secd,edf->secf/dot_general | solution.py:55
  109.2 20.8 %all-to-all-done.1 = bf16[4,512,256]{2,1,0:T(8,128)(2,1)S(1)} async-done(((bf16[4,512,256]{2,1,0:T(8,128)(2,1)}), bf16[4,512,256]{2,1,0:T(8,128)(2,1)S(1)}, u32[]{:S(2)}, u32[]{:S(2)}) %all-to-all-start.1) | async-done | bytes 1048608 | tf_op jit(solution)/shard_map/all_to_all | solution.py:12
  130.1 4.5 %fusion.6 = bf16[4,256,256]{1,2,0:T(8,128)(2,1)} fusion(bf16[2048,256,1]{1,0,2:T(8,128)(2,1)S(1)} %bitcast.80, bf16[4,256,2048]{2,1,0:T(8,128)(2,1)} %all-gather.3.cloned.1.call-done, f32[4,1,256,256]{2,3,0,1:T(8,128)S(1)} %fusion.3, f32[4,256]{1,0:T(4,128)S(1)} %bitcast.92, f32[4,256]{1,0:T(4,128)S(1)} %bitcast.90), kind=kOutput, calls=%fused_computation.17 | convolution fusion | flops 1075838976 | bytes 6823936 | tf_op jit(solution)/shard_map/secd,edf->secf/dot_general | solution.py:56
  134.6 3.5 %all-to-all-start.5 = ((bf16[4,256,256]{1,2,0:T(8,128)(2,1)}), bf16[4,256,256]{1,2,0:T(8,128)(2,1)S(1)}, u32[]{:S(2)}, u32[]{:S(2)}) async-start(bf16[4,256,256]{1,2,0:T(8,128)(2,1)} %fusion.6), calls=%async_computation.5 | async-start | bytes 1048576 | tf_op jit(solution)/shard_map/all_to_all | solution.py:65
  138.1 14.0 %all-to-all-done.5 = bf16[4,256,256]{1,2,0:T(8,128)(2,1)S(1)} async-done(((bf16[4,256,256]{1,2,0:T(8,128)(2,1)}), bf16[4,256,256]{1,2,0:T(8,128)(2,1)S(1)}, u32[]{:S(2)}, u32[]{:S(2)}) %all-to-all-start.5) | async-done | bytes 524320 | tf_op jit(solution)/shard_map/all_to_all | solution.py:65
  152.3 2.0 %gather_fusion.1 = bf16[512,256]{1,0:T(8,128)(2,1)S(1)} fusion(bf16[1024,256]{1,0:T(8,128)(2,1)S(1)} %bitcast.77, s32[1024]{0:T(1024)S(1)} %pad_clamp_fusion), kind=kCustom, calls=%fused_computation.2 | custom fusion | bytes 526336 | tf_op jit(solution)/shard_map/gather | solution.py:66
  154.2 0.8 reshape.181
  155.0 1.0 copy.46
  156.0 1.0 copy.47
  (45 shorter events, 5.2 us)
Async XLA Ops:
  7.2 98.6 %all-gather.3.cloned.1.call-start = ((), (), s32[]{:S(2)}) async-start(), calls=%async_computation.6 | async-start | bytes 5242880 | tf_op jit(solution)/shard_map/all_gather | solution.py:54
  12.2 37.1 %copy-start.1 = (f32[256,2]{0,1:T(2,128)S(1)}, f32[256,2]{0,1:T(2,128)}, u32[]{:S(2)}) copy-start(f32[256,2]{0,1:T(2,128)} %param.11) | copy-start | bytes 6148
  12.2 44.9 %copy-start = (bf16[256,2048]{1,0:T(8,128)(2,1)S(1)}, bf16[256,2048]{1,0:T(8,128)(2,1)}, u32[]{:S(2)}) copy-start(bf16[256,2048]{1,0:T(8,128)(2,1)} %param.6) | copy-start | bytes 3145732
  49.3 20.5 %copy-start.2 = (f32[512]{0:T(512)S(1)}, f32[512]{0:T(512)}, u32[]{:S(2)}) copy-start(f32[512]{0:T(512)} %param.7) | copy-start | bytes 6148
  53.9 10.8 %all-to-all-start.2 = ((bf16[4,2,128]{2,1,0:T(2,128)(2,1)}), bf16[4,2,128]{2,1,0:T(2,128)(2,1)S(1)}, u32[]{:S(2)}, u32[]{:S(2)}) async-start(bf16[4,2,128]{2,1,0:T(2,128)(2,1)} %reshape.249), calls=%async_computation.2 | async-start | bytes 4096 | tf_op jit(solution)/shard_map/all_to_all | solution.py:48
  64.7 10.5 %all-to-all-start.4 = ((bf16[4,2,128]{2,1,0:T(2,128)(2,1)}), bf16[4,2,128]{2,1,0:T(2,128)(2,1)S(1)}, u32[]{:S(2)}, u32[]{:S(2)}) async-start(bf16[4,2,128]{2,1,0:T(2,128)(2,1)} %reshape.247), calls=%async_computation.4 | async-start | bytes 4096 | tf_op jit(solution)/shard_map/all_to_all | solution.py:45
  101.9 28.1 %all-to-all-start.1 = ((bf16[4,512,256]{2,1,0:T(8,128)(2,1)}), bf16[4,512,256]{2,1,0:T(8,128)(2,1)S(1)}, u32[]{:S(2)}, u32[]{:S(2)}) async-start(bf16[4,512,256]{2,1,0:T(8,128)(2,1)} %get-tuple-element.3), calls=%async_computation.1 | async-start | bytes 2097152 | tf_op jit(solution)/shard_map/all_to_all | solution.py:12
  134.6 17.5 %all-to-all-start.5 = ((bf16[4,256,256]{1,2,0:T(8,128)(2,1)}), bf16[4,256,256]{1,2,0:T(8,128)(2,1)S(1)}, u32[]{:S(2)}, u32[]{:S(2)}) async-start(bf16[4,256,256]{1,2,0:T(8,128)(2,1)} %fusion.6), calls=%async_computation.5 | async-start | bytes 1048576 | tf_op jit(solution)/shard_map/all_to_all | solution.py:65
Sparse Core Ops, SparseCore 0:
  49.4 33.5 all-gather.2
where the time goes:
time: 164 us
  blocking collectives  58.7 us (36%)
  waiting for transfers between devices  36.8 us (22%)
  local copies, waits for them, and re-layouts  23.1 us (14%)
  starting transfers between devices  15.5 us (9%)
  between operations  14.3 us (9%)
  matrix products  7.99 us (5%)
  other arithmetic  7.42 us (5%)
    all_to_all x1, blocking collectives, on_device(): lax.all_to_all(row_buf, 'fs', split_axis=0, concat_axis=0, tiled=True)  32 us
    all_to_all x1, blocking collectives, on_device(): lax.all_to_all(folded_gate, 'fs', split_axis=0, concat_axis=1, tiled=True)  26.7 us
    all_to_all x1, waiting for transfers between devices, on_device(): lax.all_to_all(folded_up, 'fs', split_axis=0, concat_axis=1, tiled=True)  20.8 us
    all_to_all x1, waiting for transfers between devices, on_device(): lax.all_to_all(hidden_rows, 'fs', split_axis=0, concat_axis=0, tiled=True)  14 us
    all_to_all x1, starting transfers between devices, on_device(): lax.all_to_all(scale_buf.astype(jnp.bfloat16), 'fs', split_axis=0, concat...  5.05 us
    scatter x1, local copies, waits for them, and re-layouts, on_device(): jnp.zeros((total, narrow), jnp.bfloat16).at[target].set(own_cols[owner])  5.05 us
    dot_general x1, matrix products, on_device(): jnp.einsum('secd,edf->secf', piece, new_up, preferred_element_type=jnp.fl...  4.48 us
    unnamed x15, local copies, waits for them, and re-layouts  3.97 us
  transfers between devices with their start and end apart: 5, of which 3 were waited for; matrix products, arithmetic and copies ran while one was open for 12% of the time, Pallas kernels for 0%

commit v1 on v0

--- a/solution.py
+++ b/solution.py
@@ -2,6 +2,28 @@
 import jax.numpy as jnp
 from jax import lax
 from jax.sharding import PartitionSpec as P
+
+
+def split_up(shard, dim, length):
+    before, after = (shard.shape[:dim], shard.shape[dim + 1 :])
+    return jnp.moveaxis(shard.reshape(*before, length, -1, *after), dim, 0)
+
+
+def laid_out(blocks, dim):
+    lengths = list(blocks.shape[1:])
+    lengths[dim] *= blocks.shape[0]
+    return jnp.moveaxis(blocks, 0, dim).reshape(lengths)
+
+
+def exchange_directly(x, axis, split_dim, concat_dim):
+    devices, index = (lax.axis_size(axis), lax.axis_index(axis))
+    blocks = split_up(x, split_dim, devices)
+    outs = [blocks[index]]
+    for lap in range(1, devices):
+        sent = blocks[(index + lap) % devices]
+        outs.append(lax.ppermute(sent, axis, [(i, (i + lap) % devices) for i in range(devices)]))
+    blocks = jnp.stack(outs)[(index - jnp.arange(devices)) % devices]
+    return laid_out(blocks, concat_dim)
 
 
 def on_device(tokens, norm_gain, gate_master, up_master, chosen, affinity):
@@ -41,7 +63,7 @@
     row_buf = jnp.zeros((total, narrow), jnp.bfloat16).at[target].set(own_cols[owner])
     row_buf = row_buf.reshape(experts_all, capacity, narrow)
     got_rows, got_scale, got_share = (
-        lax.all_to_all(row_buf, "fs", split_axis=0, concat_axis=0, tiled=True),
+        exchange_directly(row_buf, "fs", 0, 0),
         lax.all_to_all(
             scale_buf.astype(jnp.bfloat16), "fs", split_axis=0, concat_axis=0, tiled=True
         ).astype(scale_buf.dtype),

time: 164 us -> 163 us (level)
  blocking collectives: 58.7 us -> 26.9 us
  waiting for transfers between devices: 36.8 us -> 58.2 us
  starting transfers between devices: 15.5 us -> 22.5 us
  local copies, waits for them, and re-layouts: 23.1 us -> 24.8 us
    all_to_all x1 -> x0, blocking collectives: 32 us -> none  [on_device(): lax.all_to_all(row_buf, 'fs', split_axis=0, concat_axis=0, tiled=True)]
    ppermute x0 -> x3, waiting for transfers between devices: none -> 21.3 us  [exchange_directly(): lax.ppermute(sent, axis, [(i, (i + lap) % devices) for i in range(devices)])]
    ppermute x0 -> x3, starting transfers between devices: none -> 6.14 us  [exchange_directly(): lax.ppermute(sent, axis, [(i, (i + lap) % devices) for i in range(devices)])]
  transfers between devices with their start and end apart: 5 -> 8, of which waited for: 3 -> 5; matrix products, arithmetic and copies ran while one was open for 12% -> 12% of each run, Pallas kernels for 0% -> 0%
where the time goes in v1:
time: 163 us; the launch traced here: 162 us
  waiting for transfers between devices  58.2 us (36%)
  blocking collectives  26.9 us (17%)
  local copies, waits for them, and re-layouts  24.8 us (15%)
  starting transfers between devices  22.5 us (14%)
  between operations  14.3 us (9%)
  matrix products  8.01 us (5%)
  other arithmetic  7.53 us (5%)
    all_to_all x1, blocking collectives, on_device(): lax.all_to_all(folded_gate, 'fs', split_axis=0, concat_axis=1, tiled=True)  26.9 us
    ppermute x3, waiting for transfers between devices, exchange_directly(): lax.ppermute(sent, axis, [(i, (i + lap) % devices) for i in range(devices)])  21.3 us
    all_to_all x1, waiting for transfers between devices, on_device(): lax.all_to_all(folded_up, 'fs', split_axis=0, concat_axis=1, tiled=True)  20.9 us
    all_to_all x1, waiting for transfers between devices, on_device(): lax.all_to_all(hidden_rows, 'fs', split_axis=0, concat_axis=0, tiled=True)  14 us
    ppermute x3, starting transfers between devices, exchange_directly(): lax.ppermute(sent, axis, [(i, (i + lap) % devices) for i in range(devices)])  6.14 us
    all_to_all x1, starting transfers between devices, on_device(): lax.all_to_all(scale_buf.astype(jnp.bfloat16), 'fs', split_axis=0, concat...  5.09 us
    scatter x1, local copies, waits for them, and re-layouts, on_device(): jnp.zeros((total, narrow), jnp.bfloat16).at[target].set(own_cols[owner])  5.05 us
    dot_general x1, matrix products, on_device(): jnp.einsum('secd,edf->secf', piece, new_up, preferred_element_type=jnp.fl...  4.49 us
  transfers between devices with their start and end apart: 8, of which 5 were waited for; matrix products, arithmetic and copies ran while one was open for 12% of the time, Pallas kernels for 0%

profile of v1, /device:TPU:0, one launch (start us, length us, event | category | flops | bytes accessed | tf_op | source)
XLA Modules:
  0.0 162.3 jit_solution(3044028011890907987)
XLA Ops:
  9.3 1.2 reduce-window.6
  11.3 1.0 constant_dynamic-slice_fusion.1
  12.3 5.0 %scatter_custom_fusion.1 = bf16[1024,512]{1,0:T(8,128)(2,1)S(1)} fusion(s32[512]{0:T(512)S(1)} %bitcast.99, bf16[256,512]{1,0:T(8,128)(2,1)S(1)} %constant_dynamic-slice_fusion.1, s32[1024]{0:T(1024)S(1)} %pad_clamp_fusion.2, bf16[]{:T(256)} %constant.58.clone.1), kind=kCustom, calls=%fused_computation.20 | custom fusion | bytes 1048578 | tf_op jit(solution)/shard_map/scatter | solution.py:63
  17.4 5.1 %collective-permute-start.2 = (bf16[1,256,512]{2,1,0:T(8,128)(2,1)S(1)}, bf16[1,256,512]{2,1,0:T(8,128)(2,1)S(1)}, u32[]{:S(2)}, u32[]{:S(2)}) collective-permute-start(bf16[1,256,512]{2,1,0:T(8,128)(2,1)S(1)} %get-tuple-element.4), channel_id=1, source_target_pairs={{0,12},{4,0},{8,4},{12,8},{1,13},{5,1},{9,5},{13,9},{2,14},{6,2},{... | collective-permute-start | bytes 786440 | tf_op jit(solution)/shard_map/ppermute | solution.py:24
  22.6 1.0 collective-permute-start
  23.6 5.7 %collective-permute-done.2 = bf16[1,256,512]{2,1,0:T(8,128)(2,1)S(1)} collective-permute-done((bf16[1,256,512]{2,1,0:T(8,128)(2,1)S(1)}, bf16[1,256,512]{2,1,0:T(8,128)(2,1)S(1)}, u32[]{:S(2)}, u32[]{:S(2)}) %collective-permute-start.2) | collective-permute-done | bytes 262176 | tf_op jit(solution)/shard_map/ppermute | solution.py:24
  29.3 15.6 %collective-permute-done.1 = bf16[1,256,512]{2,1,0:T(8,128)(2,1)S(1)} collective-permute-done((bf16[1,256,512]{2,1,0:T(8,128)(2,1)S(1)}, bf16[1,256,512]{2,1,0:T(8,128)(2,1)S(1)}, u32[]{:S(2)}, u32[]{:S(2)}) %collective-permute-start.1) | collective-permute-done | bytes 262176 | tf_op jit(solution)/shard_map/ppermute | solution.py:24
  45.0 1.6 gather_fusion
  47.0 2.4 %scatter_custom_fusion = f32[1024]{0:T(1024)S(1)} fusion(s32[512]{0:T(512)S(1)} %bitcast.100, f32[512]{0:T(512)S(1)} %reshape.263, f32[]{:T(128)} %constant.54.clone.1), kind=kCustom, calls=%fused_computation.47 | custom fusion | bytes 4100 | tf_op jit(solution)/shard_map/scatter | solution.py:58
  51.2 4.1 %all-to-all-start.2 = ((bf16[4,2,128]{2,1,0:T(2,128)(2,1)}), bf16[4,2,128]{2,1,0:T(2,128)(2,1)S(1)}, u32[]{:S(2)}, u32[]{:S(2)}) async-start(bf16[4,2,128]{2,1,0:T(2,128)(2,1)} %reshape.300), calls=%async_computation.2 | async-start | bytes 4096 | tf_op jit(solution)/shard_map/all_to_all | solution.py:70
  55.6 3.5 %gather_fusion.1 = f32[512]{0:T(512)S(1)} fusion(f32[256]{0:T(256)S(1)} %add_rsqrt_fusion, s32[1024]{0:T(1024)S(1)} %pad_clamp_fusion.2), kind=kCustom, calls=%fused_computation.2 | custom fusion | bytes 6144 | tf_op jit(solution)/shard_map/gather | solution.py:53
  59.1 2.4 %scatter_custom_fusion.2 = f32[1024]{0:T(1024)S(1)} fusion(s32[512]{0:T(512)S(1)} %bitcast.101, f32[512]{0:T(512)S(1)} %gather_fusion.1, f32[]{:T(128)} %constant.54.clone.1), kind=kCustom, calls=%fused_computation.45 | custom fusion | bytes 4100 | tf_op jit(solution)/shard_map/scatter | solution.py:53
  62.8 5.1 %all-to-all-start.3 = ((bf16[4,2,128]{2,1,0:T(2,128)(2,1)}), bf16[4,2,128]{2,1,0:T(2,128)(2,1)S(1)}, u32[]{:S(2)}, u32[]{:S(2)}) async-start(bf16[4,2,128]{2,1,0:T(2,128)(2,1)} %reshape.298), calls=%async_computation.3 | async-start | bytes 4096 | tf_op jit(solution)/shard_map/all_to_all | solution.py:67
  67.9 3.5 %multiply_convert_fusion = (bf16[4,512,256]{2,1,0:T(8,128)(2,1)}, bf16[4,512,256]{2,1,0:T(8,128)(2,1)S(1)}) fusion(f32[4,512,256]{2,1,0:T(8,128)} %param.9, f32[512]{0:T(512)S(1)} %copy-done.2, f32[4,512,256]{2,1,0:T(8,128)} %param.8), kind=kLoop, calls=%fused_computation.8 | loop fusion | flops 2097152 | bytes 6293504 | tf_op jit(solution)/shard_map/convert_element_type | solution.py:31
  71.4 2.0 %all-to-all-done.3 = bf16[4,2,128]{2,1,0:T(2,128)(2,1)S(1)} async-done(((bf16[4,2,128]{2,1,0:T(2,128)(2,1)}), bf16[4,2,128]{2,1,0:T(2,128)(2,1)S(1)}, u32[]{:S(2)}, u32[]{:S(2)}) %all-to-all-start.3) | async-done | bytes 2080 | tf_op jit(solution)/shard_map/all_to_all | solution.py:67
  73.4 26.9 %all_to_all.41 = bf16[4,512,256]{2,1,0:T(8,128)(2,1)S(1)} all-to-all(bf16[4,512,256]{2,1,0:T(8,128)(2,1)S(1)} %get-tuple-element.8), channel_id=1, replica_groups=mesh['grp'=2,'fs'=4,'tp'=4] {'fs'}, dimensions={0} | all-to-all | bytes 2097152 | tf_op jit(solution)/shard_map/all_to_all | solution.py:33
  100.4 3.7 %all-to-all-start.1 = ((bf16[4,512,256]{2,1,0:T(8,128)(2,1)}), bf16[4,512,256]{2,1,0:T(8,128)(2,1)S(1)}, u32[]{:S(2)}, u32[]{:S(2)}) async-start(bf16[4,512,256]{2,1,0:T(8,128)(2,1)} %get-tuple-element.7), calls=%async_computation.1 | async-start | bytes 2097152 | tf_op jit(solution)/shard_map/all_to_all | solution.py:34
  104.2 3.5 %fusion.3 = f32[4,1,256,256]{2,3,0,1:T(8,128)S(1)} fusion(bf16[2048,256,1]{1,0,2:T(8,128)(2,1)S(1)} %bitcast.92, bf16[4,256,2048]{2,1,0:T(8,128)(2,1)} %all-gather.3.cloned.1.call-done, f32[4,256]{1,0:T(4,128)S(1)} %bitcast.107), kind=kOutput, calls=%fused_computation.15 | convolution fusion | flops 1074003968 | bytes 6295552 | tf_op jit(solution)/shard_map/secd,edf->secf/dot_general | solution.py:77
  107.7 20.9 %all-to-all-done.1 = bf16[4,512,256]{2,1,0:T(8,128)(2,1)S(1)} async-done(((bf16[4,512,256]{2,1,0:T(8,128)(2,1)}), bf16[4,512,256]{2,1,0:T(8,128)(2,1)S(1)}, u32[]{:S(2)}, u32[]{:S(2)}) %all-to-all-start.1) | async-done | bytes 1048608 | tf_op jit(solution)/shard_map/all_to_all | solution.py:34
  128.6 4.5 %fusion.6 = bf16[4,256,256]{1,2,0:T(8,128)(2,1)} fusion(bf16[2048,256,1]{1,0,2:T(8,128)(2,1)S(1)} %bitcast.94, bf16[4,256,2048]{2,1,0:T(8,128)(2,1)} %all-gather.3.cloned.1.call-done, f32[4,1,256,256]{2,3,0,1:T(8,128)S(1)} %fusion.3, f32[4,256]{1,0:T(4,128)S(1)} %bitcast.108, f32[4,256]{1,0:T(4,128)S(1)} %bitcast.106), kind=kOutput, calls=%fused_computation.18 | convolution fusion | flops 1075838976 | bytes 6823936 | tf_op jit(solution)/shard_map/secd,edf->secf/dot_general | solution.py:78
  133.0 3.5 %all-to-all-start.4 = ((bf16[4,256,256]{1,2,0:T(8,128)(2,1)}), bf16[4,256,256]{1,2,0:T(8,128)(2,1)S(1)}, u32[]{:S(2)}, u32[]{:S(2)}) async-start(bf16[4,256,256]{1,2,0:T(8,128)(2,1)} %fusion.6), calls=%async_computation.4 | async-start | bytes 1048576 | tf_op jit(solution)/shard_map/all_to_all | solution.py:87
  136.5 14.0 %all-to-all-done.4 = bf16[4,256,256]{1,2,0:T(8,128)(2,1)S(1)} async-done(((bf16[4,256,256]{1,2,0:T(8,128)(2,1)}), bf16[4,256,256]{1,2,0:T(8,128)(2,1)S(1)}, u32[]{:S(2)}, u32[]{:S(2)}) %all-to-all-start.4) | async-done | bytes 524320 | tf_op jit(solution)/shard_map/all_to_all | solution.py:87
  150.7 2.0 %gather_fusion.2 = bf16[512,256]{1,0:T(8,128)(2,1)S(1)} fusion(bf16[1024,256]{1,0:T(8,128)(2,1)S(1)} %bitcast.90, s32[1024]{0:T(1024)S(1)} %pad_clamp_fusion), kind=kCustom, calls=%fused_computation.3 | custom fusion | bytes 526336 | tf_op jit(solution)/shard_map/gather | solution.py:88
  153.5 1.0 copy.46
  (54 shorter events, 8.8 us)
Async XLA Ops:
  7.2 97.0 %all-gather.3.cloned.1.call-start = ((), (), s32[]{:S(2)}) async-start(), calls=%async_computation.5 | async-start | bytes 5242880 | tf_op jit(solution)/shard_map/all_gather | solution.py:76
  17.4 11.9 %collective-permute-start.2 = (bf16[1,256,512]{2,1,0:T(8,128)(2,1)S(1)}, bf16[1,256,512]{2,1,0:T(8,128)(2,1)S(1)}, u32[]{:S(2)}, u32[]{:S(2)}) collective-permute-start(bf16[1,256,512]{2,1,0:T(8,128)(2,1)S(1)} %get-tuple-element.4), channel_id=1, source_target_pairs={{0,12},{4,0},{8,4},{12,8},{1,13},{5,1},{9,5},{13,9},{2,14},{6,2},{... | collective-permute-start | bytes 786440 | tf_op jit(solution)/shard_map/ppermute | solution.py:24
  22.6 22.3 %collective-permute-start.1 = (bf16[1,256,512]{2,1,0:T(8,128)(2,1)S(1)}, bf16[1,256,512]{2,1,0:T(8,128)(2,1)S(1)}, u32[]{:S(2)}, u32[]{:S(2)}) collective-permute-start(bf16[1,256,512]{2,1,0:T(8,128)(2,1)S(1)} %get-tuple-element.5), channel_id=1, source_target_pairs={{0,8},{4,12},{8,0},{12,4},{1,9},{5,13},{9,1},{13,5},{2,10},{6,14},... | collective-permute-start | bytes 786440 | tf_op jit(solution)/shard_map/ppermute | solution.py:24
  22.6 22.3 %collective-permute-start = (bf16[1,256,512]{2,1,0:T(8,128)(2,1)S(1)}, bf16[1,256,512]{2,1,0:T(8,128)(2,1)S(1)}, u32[]{:S(2)}, u32[]{:S(2)}) collective-permute-start(bf16[1,256,512]{2,1,0:T(8,128)(2,1)S(1)} %get-tuple-element.6), channel_id=1, source_target_pairs={{0,4},{4,8},{8,12},{12,0},{1,5},{5,9},{9,13},{13,1},{2,6},{6,10},{... | collective-permute-start | bytes 786440 | tf_op jit(solution)/shard_map/ppermute | solution.py:24
  45.0 1.6 %copy-start.1 = (f32[256,2]{0,1:T(2,128)S(1)}, f32[256,2]{0,1:T(2,128)}, u32[]{:S(2)}) copy-start(f32[256,2]{0,1:T(2,128)} %param.11) | copy-start | bytes 6148
  45.0 10.3 %copy-start = (bf16[256,2048]{1,0:T(8,128)(2,1)S(1)}, bf16[256,2048]{1,0:T(8,128)(2,1)}, u32[]{:S(2)}) copy-start(bf16[256,2048]{1,0:T(8,128)(2,1)} %param.6) | copy-start | bytes 3145732
  46.6 21.3 %copy-start.2 = (f32[512]{0:T(512)S(1)}, f32[512]{0:T(512)}, u32[]{:S(2)}) copy-start(f32[512]{0:T(512)} %param.7) | copy-start | bytes 6148
  51.2 11.6 %all-to-all-start.2 = ((bf16[4,2,128]{2,1,0:T(2,128)(2,1)}), bf16[4,2,128]{2,1,0:T(2,128)(2,1)S(1)}, u32[]{:S(2)}, u32[]{:S(2)}) async-start(bf16[4,2,128]{2,1,0:T(2,128)(2,1)} %reshape.300), calls=%async_computation.2 | async-start | bytes 4096 | tf_op jit(solution)/shard_map/all_to_all | solution.py:70
  62.8 10.6 %all-to-all-start.3 = ((bf16[4,2,128]{2,1,0:T(2,128)(2,1)}), bf16[4,2,128]{2,1,0:T(2,128)(2,1)S(1)}, u32[]{:S(2)}, u32[]{:S(2)}) async-start(bf16[4,2,128]{2,1,0:T(2,128)(2,1)} %reshape.298), calls=%async_computation.3 | async-start | bytes 4096 | tf_op jit(solution)/shard_map/all_to_all | solution.py:67
  100.4 28.2 %all-to-all-start.1 = ((bf16[4,512,256]{2,1,0:T(8,128)(2,1)}), bf16[4,512,256]{2,1,0:T(8,128)(2,1)S(1)}, u32[]{:S(2)}, u32[]{:S(2)}) async-start(bf16[4,512,256]{2,1,0:T(8,128)(2,1)} %get-tuple-element.7), calls=%async_computation.1 | async-start | bytes 2097152 | tf_op jit(solution)/shard_map/all_to_all | solution.py:34
  133.0 17.5 %all-to-all-start.4 = ((bf16[4,256,256]{1,2,0:T(8,128)(2,1)}), bf16[4,256,256]{1,2,0:T(8,128)(2,1)S(1)}, u32[]{:S(2)}, u32[]{:S(2)}) async-start(bf16[4,256,256]{1,2,0:T(8,128)(2,1)} %fusion.6), calls=%async_computation.4 | async-start | bytes 1048576 | tf_op jit(solution)/shard_map/all_to_all | solution.py:87
Sparse Core Ops, SparseCore 0:
  46.8 34.8 all-gather.2
